TPU v7x, 256 devices: a 4x2x16 block of a 4x16x16 slice. The times are simulated.
256 devices in a mesh: grp: 2 (over y), fs: 16 (over z), tp: 8 (over x, core).
Axes of the slice: x: 4, y: 2, z: 16, core: 2. Of those that a mesh axis runs over, the one named last changes fastest.
The devices are a block of a 4x16x16 slice.
Arguments:
- tokens: bfloat16 [32768, 2048], P(('grp', 'fs'), 'tp'), parts along dimension 0, may hold values from -6 to 6
- mixer_gain: float32 [2048], replicated, may hold values from 0.1 to 1.9
- branch_weight: float32 [2048, 1024], P('fs', 'tp'), may hold values from -0.125 to 0.125
- gelu_weight: float32 [2048, 1024], P('fs', 'tp'), may hold values from -0.125 to 0.125
- branch_scale: float32 [16, 64], P('fs', 'tp'), may hold values from 0.5 to 2
- gelu_scale: float32 [16, 64], P('fs', 'tp'), may hold values from 0.5 to 2
- branch_taps: float32 [4, 1024], P(None, 'tp'), may hold values from -3 to 3
- recur_gate: bfloat16 [16, 64, 64], P('tp'), may hold values from -0.75 to 0.75
- input_gate: bfloat16 [16, 64, 64], P('tp'), may hold values from -0.75 to 0.75
- decay_param: float32 [1024], P('tp'), may hold values from 4 to 7
- out_weight: float32 [1024, 2048], P('tp', 'fs'), may hold values from -0.5 to 0.5
- out_scale: float32 [16, 128], P('fs'), may hold values from 0.5 to 2
- ffn_gain: float32 [2048], replicated, may hold values from 0.1 to 1.9
- upgate_weight: float32 [2048, 5632], P('fs', 'tp'), may hold values from -0.125 to 0.125
- upval_weight: float32 [2048, 5632], P('fs', 'tp'), may hold values from -0.125 to 0.125
- upgate_scale: float32 [16, 352], P('fs', 'tp'), may hold values from 0.5 to 2
- upval_scale: float32 [16, 352], P('fs', 'tp'), may hold values from 0.5 to 2
- upgate_taps: float32 [3, 5632], P(None, 'tp'), may hold values from -3 to 3
- upval_taps: float32 [3, 5632], P(None, 'tp'), may hold values from -3 to 3
- down_weight: float32 [5632, 2048], P('tp', 'fs'), may hold values from -0.15625 to 0.15625
- down_scale: float32 [16, 128], P('fs'), may hold values from 0.5 to 2
Outputs:
- layer_out: bfloat16 [32768, 2048], P(('grp', 'fs'), 'tp'), parts along dimension 0
There are 2 independent parts, one for each index of `grp`. A program takes and returns all parts, laid end to end along the dimension named above; an argument that names none is the same for every part. Nothing has to cross between parts.
All inputs are finite; a program needn't handle non-finite values.
Results may differ from a plain program's by a relative error of at most 0.024.
Values may be sent and summed in bfloat16 or wider, within the bound.
No kernel may reach another device: no remote copies, remote signals or barrier semaphores. Data moves between devices by JAX's collectives and lax.ppermute only.
A program may use at most 128 MiB of HBM per device.

v0:
```python
import jax
import jax.numpy as jnp
from jax import lax
from jax.sharding import PartitionSpec as P

SEQ_LEN = 512


def side_by_side(arrays, axis, dim, along):
    both = jnp.concatenate(arrays, axis=along)
    filled, at, outs = (lax.all_gather(both, axis, axis=dim, tiled=True), 0, [])
    for a in arrays:
        outs.append(lax.slice_in_dim(filled, at, at + a.shape[along], axis=along))
        at += a.shape[along]
    return tuple(outs)


def copy_for_each(value, axis):
    size = lax.axis_size(axis)
    return lax.all_to_all(
        jnp.broadcast_to(value[None], (size, *value.shape)), axis, 0, 0, tiled=True
    )


def in_order(blocks, dim):
    lengths = list(blocks.shape[1:])
    lengths[dim] *= blocks.shape[0]
    return jnp.moveaxis(blocks, 0, dim).reshape(lengths)


def gather_directly(value, axis, dim):
    blocks = copy_for_each(value, axis)
    return in_order(blocks, dim)


def rms_rows(values_in, norm_gain):
    values = values_in.astype(jnp.float32)
    inverse = lax.rsqrt(jnp.mean(values * values, axis=-1, keepdims=True) + 1e-06)
    return (values * inverse * norm_gain).astype(jnp.bfloat16)


def expand_scale(gathered):
    return gathered.T.reshape(-1)


def causal_mix(values, filter_taps, seq_len):
    columns = values.shape[-1]
    grouped = values.reshape(-1, seq_len, columns)
    tap_count = filter_taps.shape[0]
    padded = jnp.pad(grouped, ((0, 0), (tap_count - 1, 0), (0, 0)))
    totals = padded[:, 0:seq_len] * filter_taps[0]
    for k in range(1, tap_count):
        totals = totals + padded[:, k : k + seq_len] * filter_taps[k]
    return totals.reshape(-1, columns)


def combine_pairs(earlier, later):
    return (earlier[0] * later[0], later[0] * earlier[1] + later[1])


def run_scan(factors, inputs, seq_len):
    columns = factors.shape[-1]
    pair = (factors.reshape(-1, seq_len, columns), inputs.reshape(-1, seq_len, columns))
    _, states = lax.associative_scan(combine_pairs, pair, axis=1)
    return states.reshape(-1, columns)


def add_rows(left, weight_piece):
    return jnp.dot(left, weight_piece, preferred_element_type=jnp.float32)


def per_device(
    tokens,
    mixer_gain,
    branch_weight,
    gelu_weight,
    branch_scale,
    gelu_scale,
    branch_taps,
    recur_gate,
    input_gate,
    decay_param,
    out_weight,
    out_scale,
    ffn_gain,
    upgate_weight,
    upval_weight,
    upgate_scale,
    upval_scale,
    upgate_taps,
    upval_taps,
    down_weight,
    down_scale,
):
    scale_list = side_by_side(
        (branch_scale, gelu_scale, out_scale, upgate_scale, upval_scale, down_scale), "fs", 0, 1
    )
    mixer_scales = scale_list[:3]
    ffn_scales = scale_list[3:]
    gathered = gather_directly(tokens, "tp", 1)
    normed = rms_rows(gathered, mixer_gain)
    pieces = side_by_side(
        (branch_weight.astype(jnp.bfloat16), gelu_weight.astype(jnp.bfloat16)), "fs", 0, 1
    )
    branch = add_rows(normed, pieces[0])
    gelu_in = add_rows(normed, pieces[1])
    branch = branch * expand_scale(mixer_scales[0])
    gelu_in = gelu_in * expand_scale(mixer_scales[1])
    convolved = causal_mix(branch, branch_taps, SEQ_LEN).astype(jnp.bfloat16)
    local_blocks = recur_gate.shape[0]
    blocks = convolved.reshape(convolved.shape[0], local_blocks, recur_gate.shape[1])
    channels = convolved.shape[1]
    recur = jax.nn.sigmoid(
        jnp.einsum("rnc,ncd->rnd", blocks, recur_gate, preferred_element_type=jnp.float32).reshape(
            -1, channels
        )
    )
    input_rate = jax.nn.sigmoid(
        jnp.einsum("rnc,ncd->rnd", blocks, input_gate, preferred_element_type=jnp.float32).reshape(
            -1, channels
        )
    )
    log_decay = -8.0 * recur * jax.nn.softplus(-decay_param)
    decay_rate = jnp.exp(log_decay)
    driven = jnp.sqrt(-jnp.expm1(2.0 * log_decay)) * input_rate * convolved.astype(jnp.float32)
    states = run_scan(decay_rate, driven, SEQ_LEN)
    gated_state = (states * jax.nn.gelu(gelu_in)).astype(jnp.bfloat16)
    out_cols = expand_scale(mixer_scales[2])
    tp_count = lax.axis_size("tp")
    feature_width = tokens.shape[1]
    whole_state = gather_directly(gated_state, "tp", 1)
    row_block = gather_directly(out_weight.astype(jnp.bfloat16), "fs", 1)
    own_columns = lax.all_to_all(row_block, "tp", split_axis=1, concat_axis=0, tiled=True)
    first_feature = lax.axis_index("tp") * feature_width
    own_scales = lax.dynamic_slice_in_dim(out_cols, first_feature, feature_width, 0)
    block_rows = whole_state.shape[1] // tp_count
    mixer_sum = jnp.zeros((whole_state.shape[0], feature_width), jnp.float32)
    for index in range(tp_count):
        partial_value = (
            jnp.dot(
                whole_state[:, index * block_rows : (index + 1) * block_rows],
                own_columns[index * block_rows : (index + 1) * block_rows],
                preferred_element_type=jnp.float32,
            )
            * own_scales
        )
        mixer_sum = mixer_sum + partial_value.astype(jnp.bfloat16).astype(jnp.float32)
    hidden_state = (tokens.astype(jnp.float32) + mixer_sum).astype(jnp.bfloat16)
    gathered_ffn = gather_directly(hidden_state, "tp", 1)
    normed_ffn = rms_rows(gathered_ffn, ffn_gain)
    upgate_bf = upgate_weight.astype(jnp.bfloat16)
    upval_bf = upval_weight.astype(jnp.bfloat16)
    gate_full, value_full = side_by_side((upgate_bf, upval_bf), "fs", 0, 1)
    up_gate = jnp.dot(normed_ffn, gate_full, preferred_element_type=jnp.float32)
    up_val = jnp.dot(normed_ffn, value_full, preferred_element_type=jnp.float32)
    up_gate = up_gate * expand_scale(ffn_scales[0])
    up_val = up_val * expand_scale(ffn_scales[1])
    conv_gate = causal_mix(up_gate, upgate_taps, SEQ_LEN)
    conv_val = causal_mix(up_val, upval_taps, SEQ_LEN)
    ffn_hidden = (jax.nn.silu(conv_gate) * conv_val).astype(jnp.bfloat16)
    down_cols = expand_scale(ffn_scales[2])
    ffn_terms = (
        jnp.dot(
            ffn_hidden,
            lax.all_gather(down_weight.astype(jnp.bfloat16), "fs", axis=1, tiled=True),
            preferred_element_type=jnp.float32,
        )
        * down_cols
    ).astype(jnp.bfloat16)
    ffn_sum = lax.psum_scatter(ffn_terms, "tp", scatter_dimension=1, tiled=True).astype(jnp.float32)
    return (hidden_state.astype(jnp.float32) + ffn_sum).astype(jnp.bfloat16)


def solution(mesh):
    in_specs = (
        P(("grp", "fs"), "tp"),
        P(),
        P("fs", "tp"),
        P("fs", "tp"),
        P("fs", "tp"),
        P("fs", "tp"),
        P(None, "tp"),
        P("tp", None, None),
        P("tp", None, None),
        P("tp"),
        P("tp", "fs"),
        P("fs", None),
        P(),
        P("fs", "tp"),
        P("fs", "tp"),
        P("fs", "tp"),
        P("fs", "tp"),
        P(None, "tp"),
        P(None, "tp"),
        P("tp", "fs"),
        P("fs", None),
    )
    out_specs = P(("grp", "fs"), "tp")
    return jax.shard_map(
        per_device, mesh=mesh, in_specs=in_specs, out_specs=out_specs, check_vma=False
    )
```

profile of v0, /device:TPU:40, one launch (start us, length us, event | category | flops | bytes accessed | tf_op | source)
XLA Modules:
  0.0 379.5 jit_solution(1736366279344310207)
XLA Ops:
  6.6 0.9 convert_element_type.151
  7.5 0.9 broadcast_in_dim.10
  8.4 24.0 %all-to-all-start.2 = ((bf16[16,128,128]{1,2,0:T(8,128)(2,1)}), bf16[16,128,128]{1,2,0:T(8,128)(2,1)}, u32[]{:S(2)}, u32[]{:S(2)}) async-start(bf16[16,128,128]{1,2,0:T(8,128)(2,1)} %broadcast_in_dim.10), calls=%async_computation.2 | async-start | bytes 1048576 | tf_op jit(solution)/shard_map/all_to_all | solution.py:20
  32.4 1.2 copy.50
  33.7 27.7 %all-to-all-done.2 = bf16[16,128,128]{1,2,0:T(8,128)(2,1)} async-done(((bf16[16,128,128]{1,2,0:T(8,128)(2,1)}), bf16[16,128,128]{1,2,0:T(8,128)(2,1)}, u32[]{:S(2)}, u32[]{:S(2)}) %all-to-all-start.2) | async-done | bytes 524320 | tf_op jit(solution)/shard_map/all_to_all | solution.py:20
  61.4 2.6 broadcast_in_dim.8
  64.1 4.9 %all-to-all-start = ((bf16[8,1024,256]{1,2,0:T(8,128)(2,1)}), bf16[8,1024,256]{1,2,0:T(8,128)(2,1)}, u32[]{:S(2)}, u32[]{:S(2)}) async-start(bf16[8,1024,256]{1,2,0:T(8,128)(2,1)} %broadcast_in_dim.8), calls=%async_computation | async-start | bytes 8388608 | tf_op jit(solution)/shard_map/all_to_all | solution.py:20
  69.2 0.6 pad_maximum_fusion.3
  70.0 0.8 pad_maximum_fusion
  71.0 30.5 %all-gather = f32[16,1,360]{2,1,0:T(1,128)S(1)} all-gather(f32[1,1,360]{2,1,0:T(1,128)S(1)} %bitcast.154), channel_id=1, replica_groups=mesh['grp'=2,'fs'=16,'tp'=8] {'fs'}, dimensions={0}, use_global_device_ids=true | all-gather | bytes 24480 | tf_op jit(solution)/shard_map/all_gather | solution.py:11
  102.0 16.7 %all-to-all-done = bf16[8,1024,256]{1,2,0:T(8,128)(2,1)} async-done(((bf16[8,1024,256]{1,2,0:T(8,128)(2,1)}), bf16[8,1024,256]{1,2,0:T(8,128)(2,1)}, u32[]{:S(2)}, u32[]{:S(2)}) %all-to-all-start) | async-done | bytes 4194336 | tf_op jit(solution)/shard_map/all_to_all | solution.py:20
  118.6 3.9 %all-to-all-start.3 = ((bf16[128,8,256]{0,2,1:T(8,128)(2,1)}), bf16[128,8,256]{0,2,1:T(8,128)(2,1)S(1)}, u32[]{:S(2)}, u32[]{:S(2)}) async-start(bf16[128,8,256]{0,2,1:T(8,128)(2,1)} %bitcast.16), calls=%async_computation.3 | async-start | bytes 1048576 | tf_op jit(solution)/shard_map/all_to_all | solution.py:133
  122.5 3.1 multiply_reduce_fusion.1
  125.6 4.2 %fusion.3 = bf16[1024,2048]{0,1:T(8,128)(2,1)} fusion(f32[2048]{0:T(1024)S(1)} %copy-done.10, f32[1024]{0:T(1024)S(1)} %add_rsqrt_fusion.1, bf16[8,1024,256]{1,2,0:T(8,128)(2,1)} %all-to-all-done), kind=kLoop, calls=%fused_computation.5 | loop fusion | flops 8388608 | bytes 8400896 | tf_op jit(solution)/shard_map/convert_element_type | solution.py:39
  129.8 6.7 %all-gather.5.cloned.1.call-done = bf16[2048,256]{1,0:T(8,128)(2,1)} async-done(((bf16[128,256]{1,0:T(8,128)(2,1)}), bf16[2048,256]{1,0:T(8,128)(2,1)}) %all-gather.5.cloned.1.call-update) | async-done | bytes 1048592 | tf_op jit(solution)/shard_map/all_gather | solution.py:11
  136.5 3.6 convolution_multiply_fusion.9
  140.7 0.3 fusion.55
  141.1 0.4 div.27
  141.8 0.3 fusion.51
  142.1 0.4 div.29
  142.8 0.6 multiply_exponential_fusion
  146.6 0.8 copy-done.22
  147.4 3.5 fusion.64
  151.1 1.6 broadcast_in_dim.9
  152.7 4.3 %all-to-all-start.1 = ((bf16[8,1024,128]{1,2,0:T(8,128)(2,1)}), bf16[8,1024,128]{1,2,0:T(8,128)(2,1)S(1)}, u32[]{:S(2)}, u32[]{:S(2)}) async-start(bf16[8,1024,128]{1,2,0:T(8,128)(2,1)} %broadcast_in_dim.9), calls=%async_computation.1 | async-start | bytes 4194304 | tf_op jit(solution)/shard_map/all_to_all | solution.py:20
  157.3 26.8 %all-to-all-done.1 = bf16[8,1024,128]{1,2,0:T(8,128)(2,1)S(1)} async-done(((bf16[8,1024,128]{1,2,0:T(8,128)(2,1)}), bf16[8,1024,128]{1,2,0:T(8,128)(2,1)S(1)}, u32[]{:S(2)}, u32[]{:S(2)}) %all-to-all-start.1) | async-done | bytes 2097184 | tf_op jit(solution)/shard_map/all_to_all | solution.py:20
  184.5 0.3 fusion.36
  185.2 0.3 fusion.40
  186.5 0.6 fusion.47
  187.3 2.5 broadcast_in_dim.11
  189.9 4.9 %all-to-all-start.4 = ((bf16[8,1024,256]{1,2,0:T(8,128)(2,1)}), bf16[8,1024,256]{1,2,0:T(8,128)(2,1)}, u32[]{:S(2)}, u32[]{:S(2)}) async-start(bf16[8,1024,256]{1,2,0:T(8,128)(2,1)} %broadcast_in_dim.11), calls=%async_computation.4 | async-start | bytes 8388608 | tf_op jit(solution)/shard_map/all_to_all | solution.py:20
  194.8 0.7 convert_element_type.178
  196.4 47.9 %all-to-all-done.4 = bf16[8,1024,256]{1,2,0:T(8,128)(2,1)} async-done(((bf16[8,1024,256]{1,2,0:T(8,128)(2,1)}), bf16[8,1024,256]{1,2,0:T(8,128)(2,1)}, u32[]{:S(2)}, u32[]{:S(2)}) %all-to-all-start.4) | async-done | bytes 4194336 | tf_op jit(solution)/shard_map/all_to_all | solution.py:20
  244.3 3.1 multiply_reduce_fusion
  247.4 4.1 %fusion.1 = bf16[1024,2048]{0,1:T(8,128)(2,1)} fusion(f32[2048]{0:T(1024)S(1)} %copy-done.11, f32[1024]{0:T(1024)S(1)} %add_rsqrt_fusion, bf16[8,1024,256]{1,2,0:T(8,128)(2,1)} %all-to-all-done.4), kind=kLoop, calls=%fused_computation.2 | loop fusion | flops 8388608 | bytes 8400896 | tf_op jit(solution)/shard_map/convert_element_type | solution.py:39
  251.5 7.9 %fusion.16 = f32[1024,704]{0,1:T(8,128)} fusion(bf16[1024,2048]{0,1:T(8,128)(2,1)} %fusion.1, bf16[2048,1408]{0,1:T(8,128)(2,1)} %all-gather.7.cloned.1.call-done, f32[704]{0:T(1024)S(1)} %mul.461), kind=kOutput, calls=%fused_computation.26 | convolution fusion | flops 2953510912 | bytes 9964288 | tf_op jit(solution)/shard_map/dot_general | solution.py:154
  259.4 4.0 %reshape.117 = f32[2,512,704]{1,0,2:T(2,128)S(1)} reshape(f32[1024,704]{0,1:T(8,128)} %fusion.16) | data formatting | bytes 5767168 | tf_op jit(solution)/shard_map/reshape | solution.py:48
  263.4 9.4 %fusion.6 = f32[2,512,704]{1,0,2:T(2,128)S(1)} fusion(f32[2,512,704]{1,0,2:T(2,128)S(1)} %reshape.117, f32[704]{0:T(1024)S(1)} %get-tuple-element.6, f32[704]{0:T(1024)S(1)} %get-tuple-element.7, f32[704]{0:T(1024)S(1)} %get-tuple-element.5), kind=kLoop, calls=%fused_computation.15 | loop fusion | flops 3604480 | bytes 5775616 | tf_op jit(solution)/shard_map/add | solution.py:53
  272.8 2.3 copy.76
  275.1 0.9 copy-done.2
  276.0 4.7 %fusion.19 = f32[1024,704]{0,1:T(8,128)} fusion(bf16[1024,2048]{0,1:T(8,128)(2,1)S(1)} %copy-done.2, bf16[2048,1408]{0,1:T(8,128)(2,1)S(1)} %copy-done.21, f32[704]{0:T(1024)S(1)} %mul.474), kind=kOutput, calls=%fused_computation.27 | convolution fusion | flops 2953510912 | bytes 9965568 | tf_op jit(solution)/shard_map/dot_general | solution.py:155
  280.8 4.0 %reshape.119 = f32[2,512,704]{1,0,2:T(2,128)S(1)} reshape(f32[1024,704]{0,1:T(8,128)} %fusion.19) | data formatting | bytes 5767168 | tf_op jit(solution)/shard_map/reshape | solution.py:48
  284.7 9.7 %fusion.10 = f32[2,512,704]{1,0,2:T(2,128)S(1)} fusion(f32[2,512,704]{1,0,2:T(2,128)S(1)} %reshape.119, f32[704]{0:T(1024)S(1)} %get-tuple-element.9, f32[704]{0:T(1024)S(1)} %get-tuple-element.10, f32[704]{0:T(1024)S(1)} %get-tuple-element.8), kind=kLoop, calls=%fused_computation.19 | loop fusion | flops 3604480 | bytes 5775616 | tf_op jit(solution)/shard_map/add | solution.py:53
  294.4 2.3 copy.77
  296.7 25.5 %all-gather.9.cloned.1.call-done = bf16[704,2048]{1,0:T(8,128)(2,1)} async-done(((bf16[704,128]{1,0:T(8,128)(2,1)}), bf16[704,2048]{1,0:T(8,128)(2,1)}) %all-gather.9.cloned.1.call-update) | async-done | bytes 2883600 | tf_op jit(solution)/shard_map/all_gather | solution.py:165
  322.2 8.2 %multiply_convert_fusion = bf16[1024,2048]{1,0:T(8,128)(2,1)} fusion(bf16[704,2048]{1,0:T(8,128)(2,1)} %all-gather.9.cloned.1.call-done, f32[2048]{0:T(1024)S(1)} %mul.487, f32[1024,704]{0,1:T(8,128)} %bitcast.129, f32[1024,704]{0,1:T(8,128)S(1)} %bitcast.128), kind=kOutput, calls=%fused_computation.6 | convolution fusion | flops 2961309696 | bytes 12853248 | tf_op jit(solution)/shard_map/dot_general | solution.py:163
  330.5 40.5 %reduce-scatter.2.cloned.1.call-done = bf16[1024,256]{1,0:T(8,128)(2,1)} async-done(((bf16[1024,2048]{1,0:T(8,128)(2,1)}), bf16[1024,256]{1,0:T(8,128)(2,1)}) %reduce-scatter.2.cloned.1.call-update) | async-done | bytes 524304 | tf_op jit(solution)/shard_map/reduce_scatter | solution.py:170
  371.0 2.0 add_convert_fusion
  (202 shorter events, 7.9 us)
Async XLA Ops:
  6.5 134.2 %copy-start = (bf16[2,64,64]{2,1,0:T(8,128)(2,1)S(1)}, bf16[2,64,64]{2,1,0:T(8,128)(2,1)}, u32[]{:S(2)}) copy-start(bf16[2,64,64]{2,1,0:T(8,128)(2,1)} %param.28) | copy-start | bytes 49156
  8.4 53.0 %all-to-all-start.2 = ((bf16[16,128,128]{1,2,0:T(8,128)(2,1)}), bf16[16,128,128]{1,2,0:T(8,128)(2,1)}, u32[]{:S(2)}, u32[]{:S(2)}) async-start(bf16[16,128,128]{1,2,0:T(8,128)(2,1)} %broadcast_in_dim.10), calls=%async_computation.2 | async-start | bytes 1048576 | tf_op jit(solution)/shard_map/all_to_all | solution.py:20
  64.0 5.1 %copy-start.8 = (f32[128,128]{1,0:T(8,128)S(1)}, f32[128,128]{1,0:T(8,128)}, u32[]{:S(2)}) copy-start(f32[128,128]{1,0:T(8,128)} %param.23) | copy-start | bytes 196612
  64.0 5.1 %copy-start.9 = (f32[128,128]{1,0:T(8,128)S(1)}, f32[128,128]{1,0:T(8,128)}, u32[]{:S(2)}) copy-start(f32[128,128]{1,0:T(8,128)} %param.24) | copy-start | bytes 196612
  64.0 5.9 %copy-start.5 = (f32[128,704]{0,1:T(8,128)S(1)}, f32[128,704]{0,1:T(8,128)}, u32[]{:S(2)}) copy-start(f32[128,704]{0,1:T(8,128)} %param.34) | copy-start | bytes 1081348
  64.0 5.9 %copy-start.6 = (f32[128,704]{0,1:T(8,128)S(1)}, f32[128,704]{0,1:T(8,128)}, u32[]{:S(2)}) copy-start(f32[128,704]{0,1:T(8,128)} %param.35) | copy-start | bytes 1081348
  64.0 6.8 %copy-start.15 = (f32[1,8]{1,0:T(1,128)S(1)}, f32[1,8]{1,0:T(1,128)}, u32[]{:S(2)}) copy-start(f32[1,8]{1,0:T(1,128)} %param.25) | copy-start | bytes 100
  64.1 6.8 %copy-start.16 = (f32[1,8]{1,0:T(1,128)S(1)}, f32[1,8]{1,0:T(1,128)}, u32[]{:S(2)}) copy-start(f32[1,8]{1,0:T(1,128)} %param.26) | copy-start | bytes 100
  64.1 6.8 %copy-start.17 = (f32[1,128]{1,0:T(1,128)S(1)}, f32[1,128]{1,0:T(1,128)}, u32[]{:S(2)}) copy-start(f32[1,128]{1,0:T(1,128)} %param.32) | copy-start | bytes 1540
  64.1 6.8 %copy-start.18 = (f32[1,44]{1,0:T(1,128)S(1)}, f32[1,44]{1,0:T(1,128)}, u32[]{:S(2)}) copy-start(f32[1,44]{1,0:T(1,128)} %param.36) | copy-start | bytes 532
  64.1 6.8 %copy-start.19 = (f32[1,44]{1,0:T(1,128)S(1)}, f32[1,44]{1,0:T(1,128)}, u32[]{:S(2)}) copy-start(f32[1,44]{1,0:T(1,128)} %param.37) | copy-start | bytes 532
  64.1 6.8 %copy-start.20 = (f32[1,128]{1,0:T(1,128)S(1)}, f32[1,128]{1,0:T(1,128)}, u32[]{:S(2)}) copy-start(f32[1,128]{1,0:T(1,128)} %param.41) | copy-start | bytes 1540
  64.1 37.8 %copy-start.24 = (f32[128]{0:T(128)S(1)}, f32[128]{0:T(128)}, u32[]{:S(2)}) copy-start(f32[128]{0:T(128)} %param.30) | copy-start | bytes 1540
  64.1 37.8 %copy-start.14 = (f32[4,128]{1,0:T(4,128)S(1)}, f32[4,128]{1,0:T(4,128)}, u32[]{:S(2)}) copy-start(f32[4,128]{1,0:T(4,128)} %param.27) | copy-start | bytes 6148
  64.1 54.5 %all-to-all-start = ((bf16[8,1024,256]{1,2,0:T(8,128)(2,1)}), bf16[8,1024,256]{1,2,0:T(8,128)(2,1)}, u32[]{:S(2)}, u32[]{:S(2)}) async-start(bf16[8,1024,256]{1,2,0:T(8,128)(2,1)} %broadcast_in_dim.8), calls=%async_computation | async-start | bytes 8388608 | tf_op jit(solution)/shard_map/all_to_all | solution.py:20
  69.0 67.5 %all-gather.5.cloned.1.call-start = ((), (), s32[]{:S(2)}) async-start(), calls=%async_computation.6 | async-start | bytes 1114112 | tf_op jit(solution)/shard_map/all_gather | solution.py:11
  69.9 181.7 %all-gather.7.cloned.1.call-start = ((), (), s32[]{:S(2)}) async-start(), calls=%async_computation.7 | async-start | bytes 6127616 | tf_op jit(solution)/shard_map/all_gather | solution.py:11
  70.8 54.9 %copy-start.10 = (f32[2048]{0:T(1024)S(1)}, f32[2048]{0:T(1024)}, u32[]{:S(2)}) copy-start(f32[2048]{0:T(1024)} %param.22) | copy-start | bytes 24580
  118.6 32.5 %all-to-all-start.3 = ((bf16[128,8,256]{0,2,1:T(8,128)(2,1)}), bf16[128,8,256]{0,2,1:T(8,128)(2,1)S(1)}, u32[]{:S(2)}, u32[]{:S(2)}) async-start(bf16[128,8,256]{0,2,1:T(8,128)(2,1)} %bitcast.16), calls=%async_computation.3 | async-start | bytes 1048576 | tf_op jit(solution)/shard_map/all_to_all | solution.py:133
  140.3 1.4 copy-start.23
  146.2 1.2 copy-start.22
  152.7 31.5 %all-to-all-start.1 = ((bf16[8,1024,128]{1,2,0:T(8,128)(2,1)}), bf16[8,1024,128]{1,2,0:T(8,128)(2,1)S(1)}, u32[]{:S(2)}, u32[]{:S(2)}) async-start(bf16[8,1024,128]{1,2,0:T(8,128)(2,1)} %broadcast_in_dim.9), calls=%async_computation.1 | async-start | bytes 4194304 | tf_op jit(solution)/shard_map/all_to_all | solution.py:20
  185.2 1.3 copy-start.4
  189.9 5.0 %copy-start.7 = (f32[704,128]{1,0:T(8,128)S(1)}, f32[704,128]{1,0:T(8,128)}, u32[]{:S(2)}) copy-start(f32[704,128]{1,0:T(8,128)} %param.40) | copy-start | bytes 1081348
  189.9 6.4 %copy-start.12 = (f32[3,704]{1,0:T(4,128)S(1)}, f32[3,704]{1,0:T(4,128)}, u32[]{:S(2)}) copy-start(f32[3,704]{1,0:T(4,128)} %param.38) | copy-start | bytes 25348
  189.9 6.5 %copy-start.13 = (f32[3,704]{1,0:T(4,128)S(1)}, f32[3,704]{1,0:T(4,128)}, u32[]{:S(2)}) copy-start(f32[3,704]{1,0:T(4,128)} %param.39) | copy-start | bytes 25348
  189.9 54.4 %all-to-all-start.4 = ((bf16[8,1024,256]{1,2,0:T(8,128)(2,1)}), bf16[8,1024,256]{1,2,0:T(8,128)(2,1)}, u32[]{:S(2)}, u32[]{:S(2)}) async-start(bf16[8,1024,256]{1,2,0:T(8,128)(2,1)} %broadcast_in_dim.11), calls=%async_computation.4 | async-start | bytes 8388608 | tf_op jit(solution)/shard_map/all_to_all | solution.py:20
  194.8 52.6 %copy-start.11 = (f32[2048]{0:T(1024)S(1)}, f32[2048]{0:T(1024)}, u32[]{:S(2)}) copy-start(f32[2048]{0:T(1024)} %param.33) | copy-start | bytes 24580
  194.8 127.5 %all-gather.9.cloned.1.call-start = ((), (), s32[]{:S(2)}) async-start(), calls=%async_computation.8 | async-start | bytes 3063808 | tf_op jit(solution)/shard_map/all_gather | solution.py:165
  195.6 175.4 %reduce-scatter.2.cloned.1.call-start = ((), (), s32[]{:S(2)}) async-start(), calls=%async_computation.9 | async-start | bytes 4718592 | tf_op jit(solution)/shard_map/reduce_scatter | solution.py:170
  263.4 11.8 %copy-start.21 = (bf16[2048,1408]{0,1:T(8,128)(2,1)S(1)}, bf16[2048,1408]{0,1:T(8,128)(2,1)}, u32[]{:S(2)}) copy-start(bf16[2048,1408]{0,1:T(8,128)(2,1)} %all-gather.7.cloned.1.call-done) | copy-start | bytes 17301508
  272.8 3.2 copy-start.2
  294.4 27.8 %copy-start.3 = (f32[88,8,2,512]{3,1,2,0:T(8,128)S(1)}, f32[88,8,2,512]{3,1,2,0:T(8,128)}, u32[]{:S(2)}) copy-start(f32[88,8,2,512]{3,1,2,0:T(8,128)} %copy.76) | copy-start | bytes 8650756
  330.4 42.5 %copy-start.1 = (bf16[2,64,64]{2,1,0:T(8,128)(2,1)S(1)}, bf16[2,64,64]{2,1,0:T(8,128)(2,1)}, u32[]{:S(2)}) copy-start(bf16[2,64,64]{2,1,0:T(8,128)(2,1)} %param.28) | copy-start | bytes 49156
Sparse Core Ops, SparseCore 0:
  71.7 64.7 all-gather.4
  138.2 103.9 all-gather.6
  243.9 78.2 all-gather.8
  330.6 40.3 reduce-scatter.1
where the time goes:
time: 381 us; the launch traced here: 379 us
  waiting for transfers between devices  192 us (50%)
  starting transfers between devices  42.2 us (11%)
  other arithmetic  40 us (10%)
  matrix products  31.4 us (8%)
  blocking collectives  30.5 us (8%)
  local copies, waits for them, and re-layouts  29 us (8%)
  between operations  14.3 us (4%)
    all_to_all x4, waiting for transfers between devices, copy_for_each(): lax.all_to_all(jnp.broadcast_to(value[None], (size, *value.shape)), axis,...  119 us
    reduce_scatter x1, waiting for transfers between devices, per_device(): lax.psum_scatter(ffn_terms, 'tp', scatter_dimension=1, tiled=True)  40.5 us
    all_to_all x4, starting transfers between devices, copy_for_each(): lax.all_to_all(jnp.broadcast_to(value[None], (size, *value.shape)), axis,...  38.1 us
    all_gather x1, blocking collectives, side_by_side(): filled, at, outs = (lax.all_gather(both, axis, axis=dim, tiled=True), 0, [])  30.5 us
    all_gather x1, waiting for transfers between devices, per_device(): lax.all_gather(down_weight.astype(jnp.bfloat16), 'fs', axis=1, tiled=True)  25.5 us
    add x2, other arithmetic, causal_mix(): totals = totals + padded[:, k:k + seq_len] * filter_taps[k]  19.1 us
    convert_element_type x2, other arithmetic, rms_rows(): return (values * inverse * norm_gain).astype(jnp.bfloat16)  8.31 us
    dot_general x1, matrix products, per_device(): jnp.dot(ffn_hidden, lax.all_gather(down_weight.astype(jnp.bfloat16), 'fs'...  8.18 us
  transfers between devices with their start and end apart: 9, of which 7 were waited for; matrix products, arithmetic and copies ran while one was open for 22% of the time, Pallas kernels for 0%

commit v1 on v0

--- a/solution.py
+++ b/solution.py
@@ -4,6 +4,13 @@
 from jax.sharding import PartitionSpec as P
 
 SEQ_LEN = 512
+
+
+def gather_over(x, axis, d):
+    count = lax.axis_size(axis)
+    blocks = jnp.stack([x for _ in range(count)])
+    blocks = lax.all_to_all(blocks, axis, split_axis=0, concat_axis=0)
+    return jnp.concatenate(blocks, axis=d)
 
 
 def side_by_side(arrays, axis, dim, along):
@@ -162,7 +169,7 @@
     ffn_terms = (
         jnp.dot(
             ffn_hidden,
-            lax.all_gather(down_weight.astype(jnp.bfloat16), "fs", axis=1, tiled=True),
+            gather_over(down_weight.astype(jnp.bfloat16), "fs", 1),
             preferred_element_type=jnp.float32,
         )
         * down_cols

time: 381 us -> 487 us (1.28)
  waiting for transfers between devices: 192 us -> 321 us
  other arithmetic: 40 us -> 24.4 us
  local copies, waits for them, and re-layouts: 29 us -> 19.9 us
  starting transfers between devices: 42.2 us -> 50.4 us
  matrix products: 31.4 us -> 26.2 us
    all_gather x2, waiting for transfers between devices: 6.67 us -> 160 us  [side_by_side(): filled, at, outs = (lax.all_gather(both, axis, axis=dim, tiled=True), 0, [])]
    all_gather x1 -> x0, waiting for transfers between devices: 25.5 us -> none  [per_device(): lax.all_gather(down_weight.astype(jnp.bfloat16), 'fs', axis=1, tiled=True)]
    add x2 -> x0, other arithmetic: 19.1 us -> none  [causal_mix(): totals = totals + padded[:, k:k + seq_len] * filter_taps[k]]
    all_to_all x0 -> x1, starting transfers between devices: none -> 8.22 us  [gather_over(): blocks = lax.all_to_all(blocks, axis, split_axis=0, concat_axis=0)]
    reshape x2 -> x1, local copies, waits for them, and re-layouts: 7.97 us -> 0.87 us  [causal_mix(): grouped = values.reshape(-1, seq_len, columns)]
    unnamed x54 -> x50, local copies, waits for them, and re-layouts: 7.7 us -> 2.24 us
  transfers between devices with their start and end apart: 9 -> 9, of which waited for: 7 -> 7; matrix products, arithmetic and copies ran while one was open for 22% -> 10% of each run, Pallas kernels for 0% -> 0%
where the time goes in v1:
time: 487 us; the launch traced here: 486 us
  waiting for transfers between devices  321 us (66%)
  starting transfers between devices  50.4 us (10%)
  blocking collectives  30.5 us (6%)
  matrix products  26.2 us (5%)
  other arithmetic  24.4 us (5%)
  local copies, waits for them, and re-layouts  19.9 us (4%)
  between operations  14.3 us (3%)
    all_gather x2, waiting for transfers between devices, side_by_side(): filled, at, outs = (lax.all_gather(both, axis, axis=dim, tiled=True), 0, [])  160 us
    all_to_all x4, waiting for transfers between devices, copy_for_each(): lax.all_to_all(jnp.broadcast_to(value[None], (size, *value.shape)), axis,...  121 us
    reduce_scatter x1, waiting for transfers between devices, per_device(): lax.psum_scatter(ffn_terms, 'tp', scatter_dimension=1, tiled=True)  40.2 us
    all_to_all x4, starting transfers between devices, copy_for_each(): lax.all_to_all(jnp.broadcast_to(value[None], (size, *value.shape)), axis,...  38.1 us
    all_gather x1, blocking collectives, side_by_side(): filled, at, outs = (lax.all_gather(both, axis, axis=dim, tiled=True), 0, [])  30.5 us
  transfers between devices with their start and end apart: 9, of which 7 were waited for; matrix products, arithmetic and copies ran while one was open for 10% of the time, Pallas kernels for 0%

profile of v1, /device:TPU:40, one launch (start us, length us, event | category | flops | bytes accessed | tf_op | source)
XLA Modules:
  0.0 486.3 jit_solution(511642881625622364)
XLA Ops:
  6.6 0.9 convert_element_type.154
  7.5 0.9 broadcast_in_dim.10
  8.4 24.0 %all-to-all-start.2 = ((bf16[16,128,128]{1,2,0:T(8,128)(2,1)}), bf16[16,128,128]{1,2,0:T(8,128)(2,1)}, u32[]{:S(2)}, u32[]{:S(2)}) async-start(bf16[16,128,128]{1,2,0:T(8,128)(2,1)} %broadcast_in_dim.10), calls=%async_computation.2 | async-start | bytes 1048576 | tf_op jit(solution)/shard_map/all_to_all | solution.py:27
  32.4 1.2 copy.98
  33.7 27.8 %all-to-all-done.2 = bf16[16,128,128]{1,2,0:T(8,128)(2,1)} async-done(((bf16[16,128,128]{1,2,0:T(8,128)(2,1)}), bf16[16,128,128]{1,2,0:T(8,128)(2,1)}, u32[]{:S(2)}, u32[]{:S(2)}) %all-to-all-start.2) | async-done | bytes 524320 | tf_op jit(solution)/shard_map/all_to_all | solution.py:27
  61.4 2.6 broadcast_in_dim.8
  64.1 4.9 %all-to-all-start = ((bf16[8,1024,256]{1,2,0:T(8,128)(2,1)}), bf16[8,1024,256]{1,2,0:T(8,128)(2,1)}, u32[]{:S(2)}, u32[]{:S(2)}) async-start(bf16[8,1024,256]{1,2,0:T(8,128)(2,1)} %broadcast_in_dim.8), calls=%async_computation | async-start | bytes 8388608 | tf_op jit(solution)/shard_map/all_to_all | solution.py:27
  69.1 0.6 pad_maximum_fusion.3
  69.9 30.5 %all-gather = f32[16,1,360]{2,1,0:T(1,128)S(1)} all-gather(f32[1,1,360]{2,1,0:T(1,128)S(1)} %bitcast.158), channel_id=1, replica_groups=mesh['grp'=2,'fs'=16,'tp'=8] {'fs'}, dimensions={0}, use_global_device_ids=true | all-gather | bytes 24480 | tf_op jit(solution)/shard_map/all_gather | solution.py:18
  100.9 17.6 %all-to-all-done = bf16[8,1024,256]{1,2,0:T(8,128)(2,1)} async-done(((bf16[8,1024,256]{1,2,0:T(8,128)(2,1)}), bf16[8,1024,256]{1,2,0:T(8,128)(2,1)}, u32[]{:S(2)}, u32[]{:S(2)}) %all-to-all-start) | async-done | bytes 4194336 | tf_op jit(solution)/shard_map/all_to_all | solution.py:27
  118.5 3.9 all-to-all-start.3
  122.4 3.1 multiply_reduce_fusion.1
  125.6 4.2 fusion.3
  129.7 6.6 %all-gather.4.cloned.1.call-done = bf16[2048,256]{1,0:T(8,128)(2,1)} async-done(((bf16[128,256]{1,0:T(8,128)(2,1)}), bf16[2048,256]{1,0:T(8,128)(2,1)}) %all-gather.4.cloned.1.call-update) | async-done | bytes 1048592 | tf_op jit(solution)/shard_map/all_gather | solution.py:18
  136.4 3.6 convolution_multiply_fusion.9
  140.6 0.3 fusion.59
  141.0 0.4 div.28
  141.6 0.3 fusion.55
  142.0 0.4 div.30
  142.7 0.6 multiply_exponential_fusion
  146.5 0.8 copy-done.21
  147.3 3.5 fusion.68
  150.9 1.6 broadcast_in_dim.9
  152.6 4.4 all-to-all-start.1
  157.3 26.8 %all-to-all-done.1 = bf16[8,1024,128]{1,2,0:T(8,128)(2,1)S(1)} async-done(((bf16[8,1024,128]{1,2,0:T(8,128)(2,1)}), bf16[8,1024,128]{1,2,0:T(8,128)(2,1)S(1)}, u32[]{:S(2)}, u32[]{:S(2)}) %all-to-all-start.1) | async-done | bytes 2097184 | tf_op jit(solution)/shard_map/all_to_all | solution.py:27
  184.1 0.3 fusion.38
  184.4 0.3 fusion.40
  184.8 0.3 fusion.42
  185.1 0.3 fusion.44
  185.4 0.3 fusion.46
  186.4 0.6 fusion.51
  187.2 2.6 broadcast_in_dim.11
  189.9 4.9 %all-to-all-start.4 = ((bf16[8,1024,256]{1,2,0:T(8,128)(2,1)}), bf16[8,1024,256]{1,2,0:T(8,128)(2,1)}, u32[]{:S(2)}, u32[]{:S(2)}) async-start(bf16[8,1024,256]{1,2,0:T(8,128)(2,1)} %broadcast_in_dim.11), calls=%async_computation.4 | async-start | bytes 8388608 | tf_op jit(solution)/shard_map/all_to_all | solution.py:27
  194.9 0.8 pad_maximum_fusion
  195.7 48.5 %all-to-all-done.4 = bf16[8,1024,256]{1,2,0:T(8,128)(2,1)} async-done(((bf16[8,1024,256]{1,2,0:T(8,128)(2,1)}), bf16[8,1024,256]{1,2,0:T(8,128)(2,1)}, u32[]{:S(2)}, u32[]{:S(2)}) %all-to-all-start.4) | async-done | bytes 4194336 | tf_op jit(solution)/shard_map/all_to_all | solution.py:27
  244.3 2.1 stack.2
  246.3 8.2 %all-to-all-start.5 = ((bf16[16,704,128]{2,1,0:T(8,128)(2,1)}), bf16[16,704,128]{2,1,0:T(8,128)(2,1)S(1)}, u32[]{:S(2)}, u32[]{:S(2)}) async-start(bf16[16,704,128]{2,1,0:T(8,128)(2,1)} %stack.2), calls=%async_computation.5 | async-start | bytes 5767168 | tf_op jit(solution)/shard_map/all_to_all | solution.py:12
  255.3 3.1 multiply_reduce_fusion
  258.5 4.2 fusion.1
  262.6 152.9 %all-gather.6.cloned.1.call-done = bf16[2048,1408]{0,1:T(8,128)(2,1)} async-done(((bf16[128,1408]{0,1:T(8,128)(2,1)}), bf16[2048,1408]{0,1:T(8,128)(2,1)}) %all-gather.6.cloned.1.call-update) | async-done | bytes 5767184 | tf_op jit(solution)/shard_map/all_gather | solution.py:18
  415.5 5.9 %fusion.20 = f32[1024,704]{0,1:T(8,128)S(1)} fusion(bf16[1024,2048]{0,1:T(8,128)(2,1)} %fusion.1, bf16[2048,1408]{0,1:T(8,128)(2,1)} %all-gather.6.cloned.1.call-done, f32[704]{0:T(1024)S(1)} %mul.463), kind=kOutput, calls=%fused_computation.31 | convolution fusion | flops 2953510912 | bytes 9964288 | tf_op jit(solution)/shard_map/dot_general | solution.py:161
  421.5 3.2 fusion.23
  424.7 0.9 copy_bitcast_fusion
  425.6 4.1 fusion.26
  429.7 1.4 copy.132
  431.1 6.4 %multiply_convert_fusion = bf16[1024,2048]{1,0:T(8,128)(2,1)} fusion(bf16[1024,704]{0,1:T(8,128)(2,1)} %bitcast.143, f32[2048]{0:T(1024)S(1)} %mul.489, bf16[16,704,128]{2,1,0:T(8,128)(2,1)S(1)} %all-to-all-done.5), kind=kOutput, calls=%fused_computation.6 | convolution fusion | flops 2956984320 | bytes 8527872 | tf_op jit(solution)/shard_map/dot_general | solution.py:170
  437.6 40.2 %reduce-scatter.2.cloned.1.call-done = bf16[1024,256]{1,0:T(8,128)(2,1)} async-done(((bf16[1024,2048]{1,0:T(8,128)(2,1)}), bf16[1024,256]{1,0:T(8,128)(2,1)}) %reduce-scatter.2.cloned.1.call-update) | async-done | bytes 524304 | tf_op jit(solution)/shard_map/reduce_scatter | solution.py:177
  477.8 2.0 add_convert_fusion
  (196 shorter events, 6.8 us)
Async XLA Ops:
  6.5 134.0 %copy-start = (bf16[2,64,64]{2,1,0:T(8,128)(2,1)S(1)}, bf16[2,64,64]{2,1,0:T(8,128)(2,1)}, u32[]{:S(2)}) copy-start(bf16[2,64,64]{2,1,0:T(8,128)(2,1)} %param.28) | copy-start | bytes 49156
  8.4 53.0 %all-to-all-start.2 = ((bf16[16,128,128]{1,2,0:T(8,128)(2,1)}), bf16[16,128,128]{1,2,0:T(8,128)(2,1)}, u32[]{:S(2)}, u32[]{:S(2)}) async-start(bf16[16,128,128]{1,2,0:T(8,128)(2,1)} %broadcast_in_dim.10), calls=%async_computation.2 | async-start | bytes 1048576 | tf_op jit(solution)/shard_map/all_to_all | solution.py:27
  64.0 5.1 %copy-start.7 = (f32[128,128]{1,0:T(8,128)S(1)}, f32[128,128]{1,0:T(8,128)}, u32[]{:S(2)}) copy-start(f32[128,128]{1,0:T(8,128)} %param.23) | copy-start | bytes 196612
  64.0 5.1 %copy-start.8 = (f32[128,128]{1,0:T(8,128)S(1)}, f32[128,128]{1,0:T(8,128)}, u32[]{:S(2)}) copy-start(f32[128,128]{1,0:T(8,128)} %param.24) | copy-start | bytes 196612
  64.0 5.8 %copy-start.14 = (f32[1,8]{1,0:T(1,128)S(1)}, f32[1,8]{1,0:T(1,128)}, u32[]{:S(2)}) copy-start(f32[1,8]{1,0:T(1,128)} %param.25) | copy-start | bytes 100
  64.0 5.8 %copy-start.15 = (f32[1,8]{1,0:T(1,128)S(1)}, f32[1,8]{1,0:T(1,128)}, u32[]{:S(2)}) copy-start(f32[1,8]{1,0:T(1,128)} %param.26) | copy-start | bytes 100
  64.0 5.8 %copy-start.16 = (f32[1,128]{1,0:T(1,128)S(1)}, f32[1,128]{1,0:T(1,128)}, u32[]{:S(2)}) copy-start(f32[1,128]{1,0:T(1,128)} %param.32) | copy-start | bytes 1540
  64.0 5.8 %copy-start.17 = (f32[1,44]{1,0:T(1,128)S(1)}, f32[1,44]{1,0:T(1,128)}, u32[]{:S(2)}) copy-start(f32[1,44]{1,0:T(1,128)} %param.36) | copy-start | bytes 532
  64.0 5.8 %copy-start.18 = (f32[1,44]{1,0:T(1,128)S(1)}, f32[1,44]{1,0:T(1,128)}, u32[]{:S(2)}) copy-start(f32[1,44]{1,0:T(1,128)} %param.37) | copy-start | bytes 532
  64.0 5.8 %copy-start.19 = (f32[1,128]{1,0:T(1,128)S(1)}, f32[1,128]{1,0:T(1,128)}, u32[]{:S(2)}) copy-start(f32[1,128]{1,0:T(1,128)} %param.41) | copy-start | bytes 1540
  64.0 36.8 %copy-start.23 = (f32[128]{0:T(128)S(1)}, f32[128]{0:T(128)}, u32[]{:S(2)}) copy-start(f32[128]{0:T(128)} %param.30) | copy-start | bytes 1540
  64.1 36.8 %copy-start.13 = (f32[4,128]{1,0:T(4,128)S(1)}, f32[4,128]{1,0:T(4,128)}, u32[]{:S(2)}) copy-start(f32[4,128]{1,0:T(4,128)} %param.27) | copy-start | bytes 6148
  64.1 54.5 %all-to-all-start = ((bf16[8,1024,256]{1,2,0:T(8,128)(2,1)}), bf16[8,1024,256]{1,2,0:T(8,128)(2,1)}, u32[]{:S(2)}, u32[]{:S(2)}) async-start(bf16[8,1024,256]{1,2,0:T(8,128)(2,1)} %broadcast_in_dim.8), calls=%async_computation | async-start | bytes 8388608 | tf_op jit(solution)/shard_map/all_to_all | solution.py:27
  68.9 56.6 %copy-start.9 = (f32[2048]{0:T(1024)S(1)}, f32[2048]{0:T(1024)}, u32[]{:S(2)}) copy-start(f32[2048]{0:T(1024)} %param.22) | copy-start | bytes 24580
  69.0 67.4 %all-gather.4.cloned.1.call-start = ((), (), s32[]{:S(2)}) async-start(), calls=%async_computation.7 | async-start | bytes 1114112 | tf_op jit(solution)/shard_map/all_gather | solution.py:18
  118.5 32.4 %all-to-all-start.3 = ((bf16[128,8,256]{0,2,1:T(8,128)(2,1)}), bf16[128,8,256]{0,2,1:T(8,128)(2,1)S(1)}, u32[]{:S(2)}, u32[]{:S(2)}) async-start(bf16[128,8,256]{0,2,1:T(8,128)(2,1)} %bitcast.16), calls=%async_computation.3 | async-start | bytes 1048576 | tf_op jit(solution)/shard_map/all_to_all | solution.py:140
  140.2 1.4 copy-start.22
  146.0 1.2 copy-start.21
  152.6 31.5 %all-to-all-start.1 = ((bf16[8,1024,128]{1,2,0:T(8,128)(2,1)}), bf16[8,1024,128]{1,2,0:T(8,128)(2,1)S(1)}, u32[]{:S(2)}, u32[]{:S(2)}) async-start(bf16[8,1024,128]{1,2,0:T(8,128)(2,1)} %broadcast_in_dim.9), calls=%async_computation.1 | async-start | bytes 4194304 | tf_op jit(solution)/shard_map/all_to_all | solution.py:27
  185.1 1.3 copy-start.3
  189.8 5.0 %copy-start.4 = (f32[128,704]{0,1:T(8,128)S(1)}, f32[128,704]{0,1:T(8,128)}, u32[]{:S(2)}) copy-start(f32[128,704]{0,1:T(8,128)} %param.34) | copy-start | bytes 1081348
  189.8 5.0 %copy-start.5 = (f32[128,704]{0,1:T(8,128)S(1)}, f32[128,704]{0,1:T(8,128)}, u32[]{:S(2)}) copy-start(f32[128,704]{0,1:T(8,128)} %param.35) | copy-start | bytes 1081348
  189.9 5.9 %copy-start.6 = (f32[704,128]{1,0:T(8,128)S(1)}, f32[704,128]{1,0:T(8,128)}, u32[]{:S(2)}) copy-start(f32[704,128]{1,0:T(8,128)} %param.40) | copy-start | bytes 1081348
  189.9 54.4 %all-to-all-start.4 = ((bf16[8,1024,256]{1,2,0:T(8,128)(2,1)}), bf16[8,1024,256]{1,2,0:T(8,128)(2,1)}, u32[]{:S(2)}, u32[]{:S(2)}) async-start(bf16[8,1024,256]{1,2,0:T(8,128)(2,1)} %broadcast_in_dim.11), calls=%async_computation.4 | async-start | bytes 8388608 | tf_op jit(solution)/shard_map/all_to_all | solution.py:27
  194.7 220.8 %all-gather.6.cloned.1.call-start = ((), (), s32[]{:S(2)}) async-start(), calls=%async_computation.8 | async-start | bytes 6127616 | tf_op jit(solution)/shard_map/all_gather | solution.py:18
  246.3 8.9 %copy-start.11 = (f32[3,704]{1,0:T(4,128)S(1)}, f32[3,704]{1,0:T(4,128)}, u32[]{:S(2)}) copy-start(f32[3,704]{1,0:T(4,128)} %param.39) | copy-start | bytes 25348
  246.3 8.9 %copy-start.12 = (f32[3,704]{1,0:T(4,128)S(1)}, f32[3,704]{1,0:T(4,128)}, u32[]{:S(2)}) copy-start(f32[3,704]{1,0:T(4,128)} %param.38) | copy-start | bytes 25348
  246.3 184.8 %all-to-all-start.5 = ((bf16[16,704,128]{2,1,0:T(8,128)(2,1)}), bf16[16,704,128]{2,1,0:T(8,128)(2,1)S(1)}, u32[]{:S(2)}, u32[]{:S(2)}) async-start(bf16[16,704,128]{2,1,0:T(8,128)(2,1)} %stack.2), calls=%async_computation.5 | async-start | bytes 5767168 | tf_op jit(solution)/shard_map/all_to_all | solution.py:12
  254.6 3.9 copy-start.10
  254.6 223.2 %reduce-scatter.2.cloned.1.call-start = ((), (), s32[]{:S(2)}) async-start(), calls=%async_computation.9 | async-start | bytes 4718592 | tf_op jit(solution)/shard_map/reduce_scatter | solution.py:177
  415.5 5.9 %copy-start.2 = (bf16[1024,2048]{0,1:T(8,128)(2,1)S(1)}, bf16[1024,2048]{0,1:T(8,128)(2,1)}, u32[]{:S(2)}) copy-start(bf16[1024,2048]{0,1:T(8,128)(2,1)} %fusion.1) | copy-start | bytes 12582916
  415.5 6.0 %copy-start.20 = (bf16[2048,1408]{0,1:T(8,128)(2,1)S(1)}, bf16[2048,1408]{0,1:T(8,128)(2,1)}, u32[]{:S(2)}) copy-start(bf16[2048,1408]{0,1:T(8,128)(2,1)} %all-gather.6.cloned.1.call-done) | copy-start | bytes 17301508
  437.5 42.2 %copy-start.1 = (bf16[2,64,64]{2,1,0:T(8,128)(2,1)S(1)}, bf16[2,64,64]{2,1,0:T(8,128)(2,1)}, u32[]{:S(2)}) copy-start(bf16[2,64,64]{2,1,0:T(8,128)(2,1)} %param.28) | copy-start | bytes 49156
Sparse Core Ops, SparseCore 0:
  71.6 64.7 all-gather.3
  197.3 218.1 all-gather.5
  437.7 40.0 reduce-scatter.1
